TPU v7x, 256 devices: a 4x2x16 block of a 4x16x16 slice. The times are simulated.
256 devices in a mesh: grp: 2 (over y), ep: 32 (over z, core), tp: 4 (over x).
Axes of the slice: x: 4, y: 2, z: 16, core: 2. Of those that a mesh axis runs over, the one named last changes fastest.
The devices are a block of a 4x16x16 slice.
Arguments:
- query_first: bfloat16 [24576, 512], P(('grp', 'ep'), 'tp'), parts along dimension 0, may hold values from -32 to 32
- query_second: bfloat16 [24576, 512], P(('grp', 'ep'), 'tp'), parts along dimension 0, may hold values from -32 to 32
- key_first: bfloat16 [24576, 512], P(('grp', 'ep'), 'tp'), parts along dimension 0, may hold values from -32 to 32
- key_second: bfloat16 [24576, 512], P(('grp', 'ep'), 'tp'), parts along dimension 0, may hold values from -32 to 32
- values: bfloat16 [24576, 1024], P(('grp', 'ep'), 'tp'), parts along dimension 0, may hold values from -6 to 6
- lambda_head: float32 [8], P('tp'), may hold values from 0.3 to 0.8
- head_gain: float32 [128], replicated, may hold values from 0.1 to 1.9
- out_weight: bfloat16 [1024, 2048], replicated, may hold values from -0.1875 to 0.1875
- tokens: bfloat16 [32768, 2048], P(('grp', 'ep', 'tp')), parts along dimension 0, may hold values from -6 to 6
- norm_gain: float32 [2048], replicated, may hold values from 0.1 to 1.9
- expert_ids: int32 [32768, 2], P(('grp', 'ep', 'tp')), parts along dimension 0, may hold values from 0 to 31, all different within a row; in each aligned block of 128 rows (0 to 127, 128 to 255, ...) at most 12 rows name the same one
- expert_weights: float32 [32768, 2], P(('grp', 'ep', 'tp')), parts along dimension 0, may hold values from 0.2 to 1
- expert_gate: bfloat16 [32, 2048, 1024], P('ep', None, 'tp'), may hold values from -0.125 to 0.125
- expert_up: bfloat16 [32, 2048, 1024], P('ep', None, 'tp'), may hold values from -0.125 to 0.125
- expert_down: bfloat16 [32, 1024, 2048], P('ep', 'tp'), may hold values from -0.1875 to 0.1875
- shared_gate: bfloat16 [2048, 512], P(None, 'tp'), may hold values from -0.125 to 0.125
- shared_up: bfloat16 [2048, 512], P(None, 'tp'), may hold values from -0.125 to 0.125
- shared_down: bfloat16 [512, 2048], P('tp'), may hold values from -0.25 to 0.25
Outputs:
- mixed: bfloat16 [24576, 2048], P(('grp', 'ep', 'tp')), parts along dimension 0
- expert_out: bfloat16 [32768, 2048], P(('grp', 'ep', 'tp')), parts along dimension 0
There are 2 independent parts, one for each index of `grp`. A program takes and returns all parts, laid end to end along the dimension named above; an argument that names none is the same for every part. Nothing has to cross between parts.
Inputs may be any that keep to these rules, and one draw needn't show every extreme that they name: `expert_ids`: in the rows of one device (aligned blocks of 128 rows) no expert is named by more than 12 rows, and in every draw some expert is named by exactly 12 rows of some block; each row names 2 different experts.
All inputs are finite; a program needn't handle non-finite values.
Results may differ from a plain program's by a relative error of at most 0.012.
Values may be sent and summed in bfloat16 or wider, within the bound.
A program may use at most 128 MiB of HBM per device.

v0:
```python
import jax
import jax.numpy as jnp
from jax import lax
from jax.sharding import Mesh
from jax.sharding import PartitionSpec as P

EP = ("ep_0", "ep_1")
GRP_EP = ("grp", "ep_0", "ep_1")
GRP_EP_TP = ("grp", "ep_0", "ep_1", "tp")
epsilon = 1e-06
block_limit = 1536


def sent_together(arrays, axis, dim, along):
    widths = [a.shape[along] for a in arrays]
    both = jnp.concatenate(arrays, axis=along)
    filled = lax.all_gather(both, axis, axis=dim, tiled=True)
    return tuple(jnp.split(filled, [sum(widths[:k]) for k in range(1, len(widths))], axis=along))


def in_blocks(value, dim, peers):
    before, after = (value.shape[:dim], value.shape[dim + 1 :])
    return jnp.moveaxis(value.reshape(*before, peers, -1, *after), dim, 0)


def in_order(tiles, dim):
    dims = list(tiles.shape[1:])
    dims[dim] *= tiles.shape[0]
    return jnp.moveaxis(tiles, 0, dim).reshape(dims)


def exchange_in_order(tiles, axes, order):
    dims = [lax.axis_size(a) for a in axes]
    tiles = tiles.reshape(*dims, *tiles.shape[1:])
    for k in order:
        tiles = lax.all_to_all(tiles, axes[k], split_axis=k, concat_axis=k, tiled=True)
    return tiles.reshape(-1, *tiles.shape[len(axes) :])


def two_step_exchange(value, groups, order, split_dim, concat_dim):
    peers = lax.axis_size(groups[0]) * lax.axis_size(groups[1])
    tiles = in_blocks(value, split_dim, peers)
    return in_order(exchange_in_order(tiles, groups, order), concat_dim)


def key_block(total_rows, shard_rows):
    best_rows = shard_rows
    for factor_rows in range(1, total_rows // shard_rows + 1):
        if total_rows % (factor_rows * shard_rows) == 0 and factor_rows * shard_rows <= block_limit:
            best_rows = factor_rows * shard_rows
    return best_rows


def softmax_update(states, scores, value_block):
    running_max, running_sum, accumulated = states
    new_max = jnp.maximum(running_max, jnp.max(scores, axis=-1))
    rescale = jnp.exp(running_max - new_max)
    weights = jnp.exp(scores - new_max[..., None])
    new_sum = running_sum * rescale + jnp.sum(weights, axis=-1)
    product = jnp.einsum(
        "qhk,khe->qhe",
        weights.astype(jnp.bfloat16),
        value_block,
        preferred_element_type=jnp.float32,
    )
    return (new_max, new_sum, accumulated * rescale[..., None] + product)


def shards(
    query_first,
    query_second,
    key_first,
    key_second,
    values,
    lambda_head,
    head_gain,
    out_weight,
    tokens,
    norm_gain,
    expert_ids,
    expert_weights,
    expert_gate,
    expert_up,
    expert_down,
    shared_gate,
    shared_up,
    shared_down,
):
    shard_rows, query_width = query_first.shape
    heads_here = lambda_head.shape[0]
    head_size = query_width // heads_here
    value_size = values.shape[1] // heads_here
    score_scale = head_size ** (-0.5)
    query_one = query_first.reshape(shard_rows, heads_here, head_size)
    query_two = query_second.reshape(shard_rows, heads_here, head_size)
    initial = (
        jnp.full((shard_rows, heads_here), -jnp.inf, jnp.float32),
        jnp.zeros((shard_rows, heads_here), jnp.float32),
        jnp.zeros((shard_rows, heads_here, value_size), jnp.float32),
    )
    carried = (initial, initial)
    key_one, key_two, value_piece = sent_together((key_first, key_second, values), EP, 0, 1)
    total_rows = key_one.shape[0]
    block_rows = key_block(total_rows, shard_rows)
    block_count = total_rows // block_rows
    stacked = (
        key_one.reshape(block_count, block_rows, heads_here, head_size),
        key_two.reshape(block_count, block_rows, heads_here, head_size),
        value_piece.reshape(block_count, block_rows, heads_here, value_size),
    )

    def fold_step(states, blocks):
        first_state, second_state = states
        key_a, key_b, value_block = blocks
        scores_a = (
            jnp.einsum("qhd,khd->qhk", query_one, key_a, preferred_element_type=jnp.float32)
            * score_scale
        )
        scores_b = (
            jnp.einsum("qhd,khd->qhk", query_two, key_b, preferred_element_type=jnp.float32)
            * score_scale
        )
        return (
            (
                softmax_update(first_state, scores_a, value_block),
                softmax_update(second_state, scores_b, value_block),
            ),
            None,
        )

    carried, unused = lax.scan(fold_step, carried, stacked)
    first_state, second_state = carried
    first_out = first_state[2] / first_state[1][..., None]
    second_out = second_state[2] / second_state[1][..., None]
    mixture = first_out - lambda_head[None, :, None] * second_out
    normed_heads = (
        mixture
        * lax.rsqrt(jnp.mean(mixture * mixture, axis=-1, keepdims=True) + epsilon)
        * head_gain
    )
    head_local = normed_heads.astype(jnp.bfloat16).reshape(shard_rows, heads_here * value_size)
    position_heads = lax.all_to_all(head_local, "tp", split_axis=0, concat_axis=1, tiled=True)
    mixed = jnp.dot(position_heads, out_weight, preferred_element_type=jnp.float32).astype(
        jnp.bfloat16
    )
    row_count, model_width = tokens.shape
    top_count = expert_ids.shape[1]
    ep_count = lax.axis_size(EP)
    local_experts = expert_gate.shape[0]
    expert_count = local_experts * ep_count
    capacity = max(2, row_count * top_count * 3 // (2 * expert_count))
    routed_rows = expert_count * capacity
    owner_span = routed_rows + row_count
    widened = tokens.astype(jnp.float32)
    normed = (
        widened
        * lax.rsqrt(jnp.mean(widened * widened, axis=-1, keepdims=True) + epsilon)
        * norm_gain
    ).astype(jnp.bfloat16)
    flat_ids = expert_ids.reshape(-1)
    onehot = (flat_ids[:, None] == jnp.arange(expert_count, dtype=jnp.int32)[None, :]).astype(
        jnp.int32
    )
    ranks = jnp.sum(onehot * jnp.cumsum(onehot, axis=0), axis=1) - 1
    slot_index = flat_ids * capacity + ranks
    token_index = jnp.arange(flat_ids.shape[0], dtype=jnp.int32) // top_count
    filled = jnp.full((routed_rows,), row_count, jnp.int32).at[slot_index].set(token_index)
    padded = jnp.concatenate([normed, jnp.zeros((1, model_width), jnp.bfloat16)], axis=0)
    outgoing = padded[filled].reshape(1, ep_count, local_experts * capacity, model_width)
    arrived = two_step_exchange(outgoing, ("ep_0", "ep_1"), (1, 0), 1, 1)
    local_rows = jnp.concatenate(
        [arrived.reshape(1, routed_rows, model_width), normed[None]], axis=1
    )
    gathered = lax.all_gather(local_rows, "tp", axis=0, tiled=True)
    owners = owner_span * lax.axis_size("tp") // owner_span
    routed_in = gathered[:, :routed_rows].reshape(
        owners, ep_count, local_experts, capacity, model_width
    )
    gate_value = jnp.einsum(
        "osecd,edf->osecf", routed_in, expert_gate, preferred_element_type=jnp.float32
    )
    up_value = jnp.einsum(
        "osecd,edf->osecf", routed_in, expert_up, preferred_element_type=jnp.float32
    )
    hidden = (jax.nn.silu(gate_value) * up_value).astype(jnp.bfloat16)
    routed_out = jnp.einsum(
        "osecf,efd->osecd", hidden, expert_down, preferred_element_type=jnp.float32
    )
    routed_out = routed_out.reshape(owners, routed_rows, model_width)
    shared_in = gathered[:, routed_rows:]
    shared_gate_value = jnp.einsum(
        "ord,df->orf", shared_in, shared_gate, preferred_element_type=jnp.float32
    )
    shared_up_value = jnp.einsum(
        "ord,df->orf", shared_in, shared_up, preferred_element_type=jnp.float32
    )
    shared_hidden = (jax.nn.silu(shared_gate_value) * shared_up_value).astype(jnp.bfloat16)
    shared_out = jnp.einsum(
        "orf,fd->ord", shared_hidden, shared_down, preferred_element_type=jnp.float32
    )
    kept_rows = lax.psum_scatter(
        jnp.concatenate([routed_out, shared_out], axis=1)
        .reshape(owners * owner_span, model_width)
        .astype(jnp.bfloat16),
        "tp",
        scatter_dimension=0,
        tiled=True,
    ).astype(jnp.float32)
    routed_back = (
        kept_rows[:routed_rows]
        .astype(jnp.bfloat16)
        .reshape(ep_count, local_experts * capacity, model_width)
    )
    returned = two_step_exchange(routed_back, ("ep_0", "ep_1"), (1, 0), 0, 0).reshape(
        routed_rows, model_width
    )
    picked = returned[slot_index].reshape(row_count, top_count, model_width).astype(jnp.float32)
    combined = jnp.sum(picked * expert_weights[:, :, None], axis=1) + kept_rows[routed_rows:]
    expert_out = combined.astype(jnp.bfloat16)
    return (mixed, expert_out)


def solution(mesh):
    torus = Mesh(
        mesh.devices.reshape(mesh.shape["grp"], 16, 2, mesh.shape["tp"]),
        ("grp", "ep_0", "ep_1", "tp"),
    )
    placed = (
        P(GRP_EP, "tp"),
        P(GRP_EP, "tp"),
        P(GRP_EP, "tp"),
        P(GRP_EP, "tp"),
        P(GRP_EP, "tp"),
        P("tp"),
        P(),
        P(),
        P(GRP_EP_TP, None),
        P(),
        P(GRP_EP_TP, None),
        P(GRP_EP_TP, None),
        P(EP, None, "tp"),
        P(EP, None, "tp"),
        P(EP, "tp", None),
        P(None, "tp"),
        P(None, "tp"),
        P("tp", None),
    )
    return jax.shard_map(
        shards,
        mesh=torus,
        in_specs=placed,
        out_specs=(P(GRP_EP_TP, None), P(GRP_EP_TP, None)),
        check_vma=False,
    )
```

profile of v0, /device:TPU:40, one launch (start us, length us, event | category | flops | bytes accessed | tf_op | source)
XLA Modules:
  0.0 628.7 jit_solution(13086468374661407831)
XLA Ops:
  20.6 5.1 all_to_all.39
  28.5 24.0 %all-to-all-start.2 = ((bf16[16,2,1,1,12,2048]{5,1,4,3,2,0:T(2,128)(2,1)}), bf16[16,2,1,1,12,2048]{5,1,4,3,2,0:T(2,128)(2,1)}, u32[]{:S(2)}, u32[]{:S(2)}) async-start(bf16[16,2,1,1,12,2048]{5,1,4,3,2,0:T(2,128)(2,1)} %copy.87), calls=%async_computation.2 | async-start | bytes 3145728 | tf_op jit(solution)/shard_map/all_to_all | solution.py:36
  53.6 73.3 %all-to-all-done.2 = bf16[16,2,1,1,12,2048]{5,1,4,3,2,0:T(2,128)(2,1)} async-done(((bf16[16,2,1,1,12,2048]{5,1,4,3,2,0:T(2,128)(2,1)}), bf16[16,2,1,1,12,2048]{5,1,4,3,2,0:T(2,128)(2,1)}, u32[]{:S(2)}, u32[]{:S(2)}) %all-to-all-start.2) | async-done | bytes 1572896 | tf_op jit(solution)/shard_map/all_to_all | solution.py:36
  135.2 83.4 %all-gather.5.cloned.1.call-done = bf16[4,512,2048]{2,1,0:T(8,128)(2,1)} async-done(((bf16[1,512,2048]{2,1,0:T(8,128)(2,1)}), bf16[4,512,2048]{2,1,0:T(8,128)(2,1)}) %all-gather.5.cloned.1.call-update) | async-done | bytes 8388624 | tf_op jit(solution)/shard_map/all_gather | solution.py:174
  218.6 6.5 %slice.34 = bf16[4,384,2048]{2,1,0:T(8,128)(2,1)} slice(bf16[4,512,2048]{2,1,0:T(8,128)(2,1)} %all-gather.5.cloned.1.call-done), slice={[0:4], [0:384], [0:2048]} | slice | bytes 12582912 | tf_op jit(solution)/shard_map/slice | solution.py:176
  225.1 10.4 %copy.89 = bf16[4,384,2048]{2,0,1:T(4,128)(2,1)} copy(bf16[4,384,2048]{2,1,0:T(8,128)(2,1)} %slice.34) | data formatting | bytes 12582912 | tf_op jit(solution)/shard_map/slice | solution.py:176
  235.5 11.6 %fusion.44 = f32[4,32,12,256]{3,1,2,0:T(8,128)} fusion(bf16[4,32,12,2048]{3,0,2,1:T(4,128)(2,1)} %bitcast.191, bf16[1,2048,256]{2,1,0:T(8,128)(2,1)S(1)} %copy-done.15), kind=kOutput, calls=%fused_computation.52 | convolution fusion | flops 1610612736 | bytes 8912896 | tf_op jit(solution)/shard_map/osecd,edf->osecf/dot_general | solution.py:179
  247.2 17.0 %convert_bitcast_fusion = bf16[4,32,1,12,2048]{4,1,3,0,2:T(8,128)(2,1)} fusion(bf16[1,256,2048]{2,1,0:T(8,128)(2,1)S(1)} %copy-done, bf16[4,32,12,2048]{3,0,2,1:T(4,128)(2,1)} %bitcast.192, f32[4,32,12,256]{3,1,2,0:T(8,128)} %fusion.44, bf16[1,2048,256]{2,1,0:T(8,128)(2,1)} %param.33), kind=kOutput, calls=%fused_computation.49 | convolution fusion | flops 3226730496 | bytes 16252928 | tf_op jit(solution)/shard_map/osecf,efd->osecd/dot_general | solution.py:186
  264.2 10.5 %copy.92 = bf16[4,32,1,12,2048]{4,0,3,1,2:T(4,128)(2,1)} copy(bf16[4,32,1,12,2048]{4,1,3,0,2:T(8,128)(2,1)} %convert_bitcast_fusion) | data formatting | bytes 12582912 | tf_op jit(solution)/shard_map/osecf,efd->osecd/transpose | solution.py:186
  277.1 5.3 convolution_convert_fusion
  285.7 8.4 %pad_maximum_fusion = bf16[4,512,2048]{2,0,1:T(4,128)(2,1)} fusion(bf16[4,128,2048]{2,0,1:T(4,128)(2,1)S(1)} %copy.93, bf16[4,384,2048]{2,0,1:T(4,128)(2,1)} %bitcast.190), kind=kLoop, calls=%fused_computation.48 | loop fusion | flops 4194304 | bytes 16777216 | tf_op jit(solution)/shard_map/concatenate | solution.py:202
  294.1 11.4 %copy.94 = bf16[4,512,2048]{2,1,0:T(8,128)(2,1)} copy(bf16[4,512,2048]{2,0,1:T(4,128)(2,1)} %pad_maximum_fusion) | data formatting | bytes 16777216 | tf_op jit(solution)/shard_map/concatenate | solution.py:202
  307.3 4.8 fusion.94
  312.1 11.6 %reshape.177 = bf16[8,1536,2,64]{3,2,1,0:T(2,128)(2,1)} reshape(bf16[12288,128]{1,0:T(8,128)(2,1)} %get-tuple-element.183) | data formatting | bytes 6291456 | tf_op jit(solution)/shard_map/reshape | solution.py:107
  323.8 15.5 %copy.77 = bf16[8,1536,2,64]{1,3,2,0:T(8,128)(2,1)} copy(bf16[8,1536,2,64]{3,2,1,0:T(2,128)(2,1)} %reshape.177) | data formatting | bytes 6291456
  339.2 11.6 %reshape.179 = bf16[8,1536,2,64]{3,2,1,0:T(2,128)(2,1)} reshape(bf16[12288,128]{1,0:T(8,128)(2,1)} %get-tuple-element.182) | data formatting | bytes 6291456 | tf_op jit(solution)/shard_map/reshape | solution.py:108
  350.9 15.6 %copy.79 = bf16[8,1536,2,64]{1,3,2,0:T(8,128)(2,1)} copy(bf16[8,1536,2,64]{3,2,1,0:T(2,128)(2,1)} %reshape.179) | data formatting | bytes 6291456
  366.4 6.4 %split.13 = bf16[12288,256]{1,0:T(8,128)(2,1)} slice(bf16[12288,512]{1,0:T(8,128)(2,1)} %all-gather.3.cloned.1.call-done), slice={[0:12288], [256:512]} | slice | bytes 12582912 | tf_op jit(solution)/shard_map/split | solution.py:18
  372.8 9.8 %reshape.178 = bf16[8,1536,2,128]{3,2,1,0:T(2,128)(2,1)} reshape(bf16[12288,256]{1,0:T(8,128)(2,1)} %split.13) | data formatting | bytes 12582912 | tf_op jit(solution)/shard_map/reshape | solution.py:109
  382.6 118.0 %while.21 = (s32[]{:T(128)}, f32[384,2]{0,1:T(2,128)S(1)}, f32[384,2]{0,1:T(2,128)S(1)}, f32[384,2,128]{0,2,1:T(8,128)S(1)}, f32[384,2]{0,1:T(2,128)S(1)}, /*ind...) while((s32[]{:T(128)}, f32[384,2]{0,1:T(2,128)S(1)}, ...), condition=%wide.region_5.6_spmd.clone, body=%wide.region_0.5_spmd.clone.sunk | while | flops 925441536 | bytes 92308720 | solution.py:131
  392.8 3.5 fusion.125
  407.6 3.5 fusion.125
  422.3 3.5 fusion.125
  437.0 3.5 fusion.125
  451.8 3.5 fusion.125
  466.5 3.5 fusion.125
  508.0 5.0 all_to_all.40
  513.0 4.2 all-to-all-start
  520.0 3.6 all-to-all-done
  523.6 10.7 %all-to-all-start.4 = ((bf16[16,2,1,12,2048]{4,1,3,2,0:T(2,128)(2,1)}), bf16[16,2,1,12,2048]{4,1,3,2,0:T(2,128)(2,1)S(1)}, u32[]{:S(2)}, u32[]{:S(2)}) async-start(bf16[16,2,1,12,2048]{4,1,3,2,0:T(2,128)(2,1)} %copy.96), calls=%async_computation.5 | async-start | bytes 3145728 | tf_op jit(solution)/shard_map/all_to_all | solution.py:36
  534.4 3.7 convolution_convert_fusion.1
  538.2 69.0 %all-to-all-done.4 = bf16[16,2,1,12,2048]{4,1,3,2,0:T(2,128)(2,1)S(1)} async-done(((bf16[16,2,1,12,2048]{4,1,3,2,0:T(2,128)(2,1)}), bf16[16,2,1,12,2048]{4,1,3,2,0:T(2,128)(2,1)S(1)}, u32[]{:S(2)}, u32[]{:S(2)}) %all-to-all-start.4) | async-done | bytes 1572896 | tf_op jit(solution)/shard_map/all_to_all | solution.py:36
  (245 shorter events, 153.3 us)
Async XLA Ops:
  7.2 240.0 %copy-start = (bf16[1,256,2048]{2,1,0:T(8,128)(2,1)S(1)}, bf16[1,256,2048]{2,1,0:T(8,128)(2,1)}, u32[]{:S(2)}) copy-start(bf16[1,256,2048]{2,1,0:T(8,128)(2,1)} %param.34) | copy-start | bytes 3145732
  20.6 32.0 %copy-start.5 = (bf16[128,2048]{1,0:T(8,128)(2,1)S(1)}, bf16[128,2048]{1,0:T(8,128)(2,1)}, u32[]{:S(2)}) copy-start(bf16[128,2048]{1,0:T(8,128)(2,1)} %param.28) | copy-start | bytes 1572868
  20.6 32.0 %copy-start.11 = (f32[2048]{0:T(1024)S(1)}, f32[2048]{0:T(1024)}, u32[]{:S(2)}) copy-start(f32[2048]{0:T(1024)} %param.29) | copy-start | bytes 24580
  28.5 98.3 %all-to-all-start.2 = ((bf16[16,2,1,1,12,2048]{5,1,4,3,2,0:T(2,128)(2,1)}), bf16[16,2,1,1,12,2048]{5,1,4,3,2,0:T(2,128)(2,1)}, u32[]{:S(2)}, u32[]{:S(2)}) async-start(bf16[16,2,1,1,12,2048]{5,1,4,3,2,0:T(2,128)(2,1)} %copy.87), calls=%async_computation.2 | async-start | bytes 3145728 | tf_op jit(solution)/shard_map/all_to_all | solution.py:36
  52.5 166.1 %all-gather.5.cloned.1.call-start = ((), (), s32[]{:S(2)}) async-start(), calls=%async_computation.7 | async-start | bytes 10485760 | tf_op jit(solution)/shard_map/all_gather | solution.py:174
  129.0 4.7 copy-start.6
  129.0 4.7 copy-start.7
  129.1 4.7 copy-start.8
  130.4 4.6 copy-start.9
  130.4 4.7 copy-start.10
  133.7 173.7 %all-gather.3.cloned.1.call-start = ((), (), s32[]{:S(2)}) async-start(), calls=%async_computation.6 | async-start | bytes 12976128 | tf_op jit(solution)/shard_map/all_gather | solution.py:17
  134.6 367.3 %reduce-scatter.2.cloned.1.call-start = ((), (), s32[]{:S(2)}) async-start(), calls=%async_computation.8 | async-start | bytes 10485760 | tf_op jit(solution)/shard_map/reduce_scatter | solution.py:201
  225.1 10.4 %copy-start.15 = (bf16[1,2048,256]{2,1,0:T(8,128)(2,1)S(1)}, bf16[1,2048,256]{2,1,0:T(8,128)(2,1)}, u32[]{:S(2)}) copy-start(bf16[1,2048,256]{2,1,0:T(8,128)(2,1)} %param.32) | copy-start | bytes 3145732
  264.2 10.5 %copy-start.16 = (bf16[2048,128]{1,0:T(8,128)(2,1)S(1)}, bf16[2048,128]{1,0:T(8,128)(2,1)}, u32[]{:S(2)}) copy-start(bf16[2048,128]{1,0:T(8,128)(2,1)} %param.35) | copy-start | bytes 1572868
  264.2 12.9 %copy-start.17 = (bf16[128,2048]{1,0:T(8,128)(2,1)S(1)}, bf16[128,2048]{1,0:T(8,128)(2,1)}, u32[]{:S(2)}) copy-start(bf16[128,2048]{1,0:T(8,128)(2,1)} %param.37) | copy-start | bytes 1572868
  264.2 12.9 %copy-start.18 = (bf16[2048,128]{1,0:T(8,128)(2,1)S(1)}, bf16[2048,128]{1,0:T(8,128)(2,1)}, u32[]{:S(2)}) copy-start(bf16[2048,128]{1,0:T(8,128)(2,1)} %param.36) | copy-start | bytes 1572868
  382.6 118.1 %copy-start.13 = (f32[2]{0:T(128)S(1)}, f32[2]{0:T(128)}, u32[]{:S(2)}) copy-start(f32[2]{0:T(128)} %param.25) | copy-start | bytes 28
  382.6 118.2 %copy-start.14 = (f32[128]{0:T(128)S(1)}, f32[128]{0:T(128)}, u32[]{:S(2)}) copy-start(f32[128]{0:T(128)} %param.26) | copy-start | bytes 1540
  384.7 3.0 copy-start.2
  392.8 3.8 copy-start.3
  399.5 2.9 copy-start.2
  407.6 3.8 copy-start.3
  422.3 3.8 copy-start.3
  437.0 3.8 copy-start.3
  451.8 3.8 copy-start.3
  466.5 3.8 copy-start.3
  481.2 3.8 copy-start.3
  495.9 3.8 copy-start.3
  508.0 26.3 %copy-start.12 = (f32[128,2]{0,1:T(2,128)S(1)}, f32[128,2]{0,1:T(2,128)}, u32[]{:S(2)}) copy-start(f32[128,2]{0,1:T(2,128)} %param.31) | copy-start | bytes 3076
  513.0 10.6 %all-to-all-start = ((bf16[4,96,256]{2,1,0:T(8,128)(2,1)}), bf16[4,96,256]{2,1,0:T(8,128)(2,1)S(1)}, u32[]{:S(2)}, u32[]{:S(2)}) async-start(bf16[4,96,256]{2,1,0:T(8,128)(2,1)} %all_to_all.26), calls=%async_computation | async-start | bytes 393216 | tf_op jit(solution)/shard_map/all_to_all | solution.py:142
  523.6 83.7 %all-to-all-start.4 = ((bf16[16,2,1,12,2048]{4,1,3,2,0:T(2,128)(2,1)}), bf16[16,2,1,12,2048]{4,1,3,2,0:T(2,128)(2,1)S(1)}, u32[]{:S(2)}, u32[]{:S(2)}) async-start(bf16[16,2,1,12,2048]{4,1,3,2,0:T(2,128)(2,1)} %copy.96), calls=%async_computation.5 | async-start | bytes 3145728 | tf_op jit(solution)/shard_map/all_to_all | solution.py:36
  611.8 9.9 %copy-start.1 = (bf16[1,256,2048]{2,1,0:T(8,128)(2,1)S(1)}, bf16[1,256,2048]{2,1,0:T(8,128)(2,1)}, u32[]{:S(2)}) copy-start(bf16[1,256,2048]{2,1,0:T(8,128)(2,1)} %param.34) | copy-start | bytes 3145732
  (14 other events, 34.6 us)
Sparse Core Ops, SparseCore 0:
  133.8 84.7 all-gather.4
  221.0 86.2 all-gather.2
  310.0 83.3 reduce-scatter.1
where the time goes:
time: 638 us; the launch traced here: 629 us
  waiting for transfers between devices  231 us (36%)
  local copies, waits for them, and re-layouts  189 us (30%)
  matrix products  107 us (17%)
  starting transfers between devices  39.4 us (6%)
  other arithmetic  35.5 us (6%)
  between operations  14.7 us (2%)
  blocking collectives  10.2 us (2%)
    all_to_all x2, waiting for transfers between devices, exchange_in_order(): lax.all_to_all(tiles, axes[k], split_axis=k, concat_axis=k, tiled=True)  142 us
    all_gather x1, waiting for transfers between devices, shards(): gathered = lax.all_gather(local_rows, 'tp', axis=0, tiled=True)  83.4 us
    dot_general x16, matrix products, softmax_update(): jnp.einsum('qhk,khe->qhe', weights.astype(jnp.bfloat16), value_block, pre...  35.7 us
    all_to_all x2, starting transfers between devices, exchange_in_order(): lax.all_to_all(tiles, axes[k], split_axis=k, concat_axis=k, tiled=True)  34.7 us
    unnamed x38, local copies, waits for them, and re-layouts  32.3 us
    while x64, local copies, waits for them, and re-layouts  19.1 us
    dynamic_slice x16, local copies, waits for them, and re-layouts, shards(): carried, unused = lax.scan(fold_step, carried, stacked)  17.6 us
    dot_general x1, matrix products, shards(): jnp.einsum('osecf,efd->osecd', hidden, expert_down, preferred_element_typ...  17 us
  transfers between devices with their start and end apart: 6, of which 5 were waited for; matrix products, arithmetic and copies ran while one was open for 43% of the time, Pallas kernels for 0%

commit v1 on v0

--- a/solution.py
+++ b/solution.py
@@ -171,7 +171,9 @@
     local_rows = jnp.concatenate(
         [arrived.reshape(1, routed_rows, model_width), normed[None]], axis=1
     )
-    gathered = lax.all_gather(local_rows, "tp", axis=0, tiled=True)
+    gathered = jnp.concatenate(
+        lax.all_to_all(jnp.stack([local_rows] * lax.axis_size("tp")), "tp", 0, 0), axis=0
+    )
     owners = owner_span * lax.axis_size("tp") // owner_span
     routed_in = gathered[:, :routed_rows].reshape(
         owners, ep_count, local_experts, capacity, model_width

time: 638 us -> 671 us (1.052)
  waiting for transfers between devices: 231 us -> 254 us
    all_to_all x0 -> x1, waiting for transfers between devices: none -> 92.5 us  [shards(): lax.all_to_all(jnp.stack([local_rows] * lax.axis_size('tp')), 'tp', 0, 0)]
    all_gather x1 -> x0, waiting for transfers between devices: 83.4 us -> none  [shards(): gathered = lax.all_gather(local_rows, 'tp', axis=0, tiled=True)]
    all_to_all x2, waiting for transfers between devices: 142 us -> 157 us  [exchange_in_order(): lax.all_to_all(tiles, axes[k], split_axis=k, concat_axis=k, tiled=True)]
    unnamed x38 -> x32, local copies, waits for them, and re-layouts: 32.3 us -> 32.2 us
  transfers between devices with their start and end apart: 6 -> 6, of which waited for: 5 -> 4; matrix products, arithmetic and copies ran while one was open for 43% -> 44% of each run, Pallas kernels for 0% -> 0%
where the time goes in v1:
time: 671 us; the launch traced here: 661 us
  waiting for transfers between devices  254 us (38%)
  local copies, waits for them, and re-layouts  193 us (29%)
  matrix products  107 us (16%)
  starting transfers between devices  44.3 us (7%)
  other arithmetic  35.1 us (5%)
  between operations  16.4 us (2%)
  blocking collectives  10.2 us (2%)
    all_to_all x2, waiting for transfers between devices, exchange_in_order(): lax.all_to_all(tiles, axes[k], split_axis=k, concat_axis=k, tiled=True)  157 us
    all_to_all x1, waiting for transfers between devices, shards(): lax.all_to_all(jnp.stack([local_rows] * lax.axis_size('tp')), 'tp', 0, 0)  92.5 us
    dot_general x16, matrix products, softmax_update(): jnp.einsum('qhk,khe->qhe', weights.astype(jnp.bfloat16), value_block, pre...  35.7 us
    all_to_all x2, starting transfers between devices, exchange_in_order(): lax.all_to_all(tiles, axes[k], split_axis=k, concat_axis=k, tiled=True)  34.6 us
    unnamed x32, local copies, waits for them, and re-layouts  32.2 us
    while x64, local copies, waits for them, and re-layouts  19 us
    dynamic_slice x16, local copies, waits for them, and re-layouts, shards(): carried, unused = lax.scan(fold_step, carried, stacked)  17.6 us
    dot_general x8, matrix products, fold_step(): jnp.einsum('qhd,khd->qhk', query_two, key_b, preferred_element_type=jnp.f...  17 us
  transfers between devices with their start and end apart: 6, of which 4 were waited for; matrix products, arithmetic and copies ran while one was open for 44% of the time, Pallas kernels for 0%

profile of v1, /device:TPU:40, one launch (start us, length us, event | category | flops | bytes accessed | tf_op | source)
XLA Modules:
  0.0 660.7 jit_solution(41283349972062078)
XLA Ops:
  23.4 5.1 all_to_all.44
  31.3 24.3 %all-to-all-start.2 = ((bf16[16,2,1,1,12,2048]{5,1,4,3,2,0:T(2,128)(2,1)}), bf16[16,2,1,1,12,2048]{5,1,4,3,2,0:T(2,128)(2,1)}, u32[]{:S(2)}, u32[]{:S(2)}) async-start(bf16[16,2,1,1,12,2048]{5,1,4,3,2,0:T(2,128)(2,1)} %copy.87), calls=%async_computation.2 | async-start | bytes 3145728 | tf_op jit(solution)/shard_map/all_to_all | solution.py:36
  56.6 88.0 %all-to-all-done.2 = bf16[16,2,1,1,12,2048]{5,1,4,3,2,0:T(2,128)(2,1)} async-done(((bf16[16,2,1,1,12,2048]{5,1,4,3,2,0:T(2,128)(2,1)}), bf16[16,2,1,1,12,2048]{5,1,4,3,2,0:T(2,128)(2,1)}, u32[]{:S(2)}, u32[]{:S(2)}) %all-to-all-start.2) | async-done | bytes 1572896 | tf_op jit(solution)/shard_map/all_to_all | solution.py:36
  149.9 4.3 stack.2
  154.2 5.9 all-to-all-start.3
  160.7 92.5 %all-to-all-done.3 = bf16[4,1,512,2048]{3,2,1,0:T(8,128)(2,1)} async-done(((bf16[4,1,512,2048]{3,2,1,0:T(8,128)(2,1)}), bf16[4,1,512,2048]{3,2,1,0:T(8,128)(2,1)}, u32[]{:S(2)}, u32[]{:S(2)}) %all-to-all-start.3) | async-done | bytes 8388640 | tf_op jit(solution)/shard_map/all_to_all | solution.py:175
  253.3 6.5 slice.34
  259.8 10.4 %copy.89 = bf16[4,384,2048]{2,0,1:T(4,128)(2,1)} copy(bf16[4,384,2048]{2,1,0:T(8,128)(2,1)} %slice.34) | data formatting | bytes 12582912 | tf_op jit(solution)/shard_map/slice | solution.py:178
  270.1 11.4 %fusion.44 = f32[4,32,12,256]{3,1,2,0:T(8,128)} fusion(bf16[4,32,12,2048]{3,0,2,1:T(4,128)(2,1)} %bitcast.194, bf16[1,2048,256]{2,1,0:T(8,128)(2,1)S(1)} %copy-done.12), kind=kOutput, calls=%fused_computation.52 | convolution fusion | flops 1610612736 | bytes 8912896 | tf_op jit(solution)/shard_map/osecd,edf->osecf/dot_general | solution.py:181
  281.5 16.8 %convert_bitcast_fusion = bf16[4,32,1,12,2048]{4,1,3,0,2:T(8,128)(2,1)} fusion(bf16[1,256,2048]{2,1,0:T(8,128)(2,1)S(1)} %copy-done, bf16[4,32,12,2048]{3,0,2,1:T(4,128)(2,1)} %bitcast.195, f32[4,32,12,256]{3,1,2,0:T(8,128)} %fusion.44, bf16[1,2048,256]{2,1,0:T(8,128)(2,1)} %param.33), kind=kOutput, calls=%fused_computation.49 | convolution fusion | flops 3226730496 | bytes 16252928 | tf_op jit(solution)/shard_map/osecf,efd->osecd/dot_general | solution.py:188
  298.3 10.4 %copy.92 = bf16[4,32,1,12,2048]{4,0,3,1,2:T(4,128)(2,1)} copy(bf16[4,32,1,12,2048]{4,1,3,0,2:T(8,128)(2,1)} %convert_bitcast_fusion) | data formatting | bytes 12582912 | tf_op jit(solution)/shard_map/osecf,efd->osecd/transpose | solution.py:188
  311.1 5.2 convolution_convert_fusion
  319.5 8.4 %pad_maximum_fusion = bf16[4,512,2048]{2,0,1:T(4,128)(2,1)} fusion(bf16[4,128,2048]{2,0,1:T(4,128)(2,1)S(1)} %copy.93, bf16[4,384,2048]{2,0,1:T(4,128)(2,1)} %bitcast.193), kind=kLoop, calls=%fused_computation.48 | loop fusion | flops 4194304 | bytes 16777216 | tf_op jit(solution)/shard_map/concatenate | solution.py:204
  327.9 11.3 %copy.94 = bf16[4,512,2048]{2,1,0:T(8,128)(2,1)} copy(bf16[4,512,2048]{2,0,1:T(4,128)(2,1)} %pad_maximum_fusion) | data formatting | bytes 16777216 | tf_op jit(solution)/shard_map/concatenate | solution.py:204
  339.3 4.8 fusion.94
  344.1 11.6 %reshape.184 = bf16[8,1536,2,64]{3,2,1,0:T(2,128)(2,1)} reshape(bf16[12288,128]{1,0:T(8,128)(2,1)} %get-tuple-element.183) | data formatting | bytes 6291456 | tf_op jit(solution)/shard_map/reshape | solution.py:107
  355.8 15.5 %copy.77 = bf16[8,1536,2,64]{1,3,2,0:T(8,128)(2,1)} copy(bf16[8,1536,2,64]{3,2,1,0:T(2,128)(2,1)} %reshape.184) | data formatting | bytes 6291456
  371.2 11.6 %reshape.186 = bf16[8,1536,2,64]{3,2,1,0:T(2,128)(2,1)} reshape(bf16[12288,128]{1,0:T(8,128)(2,1)} %get-tuple-element.182) | data formatting | bytes 6291456 | tf_op jit(solution)/shard_map/reshape | solution.py:108
  382.8 15.5 %copy.79 = bf16[8,1536,2,64]{1,3,2,0:T(8,128)(2,1)} copy(bf16[8,1536,2,64]{3,2,1,0:T(2,128)(2,1)} %reshape.186) | data formatting | bytes 6291456
  398.4 6.4 split.13
  404.8 9.8 %reshape.185 = bf16[8,1536,2,128]{3,2,1,0:T(2,128)(2,1)} reshape(bf16[12288,256]{1,0:T(8,128)(2,1)} %split.13) | data formatting | bytes 12582912 | tf_op jit(solution)/shard_map/reshape | solution.py:109
  414.6 118.0 %while.21 = (s32[]{:T(128)}, f32[384,2]{0,1:T(2,128)S(1)}, f32[384,2]{0,1:T(2,128)S(1)}, f32[384,2,128]{0,2,1:T(8,128)S(1)}, f32[384,2]{0,1:T(2,128)S(1)}, /*ind...) while((s32[]{:T(128)}, f32[384,2]{0,1:T(2,128)S(1)}, ...), condition=%wide.region_5.6_spmd.clone, body=%wide.region_0.5_spmd.clone.sunk | while | flops 925441536 | bytes 92308720 | solution.py:131
  424.8 3.5 fusion.125
  439.5 3.5 fusion.125
  454.2 3.5 fusion.125
  483.6 3.5 fusion.125
  513.1 3.5 fusion.125
  539.8 5.0 all_to_all.45
  551.1 3.7 all-to-all-done
  554.8 10.3 %all-to-all-start.5 = ((bf16[16,2,1,12,2048]{4,1,3,2,0:T(2,128)(2,1)}), bf16[16,2,1,12,2048]{4,1,3,2,0:T(2,128)(2,1)S(1)}, u32[]{:S(2)}, u32[]{:S(2)}) async-start(bf16[16,2,1,12,2048]{4,1,3,2,0:T(2,128)(2,1)} %copy.96), calls=%async_computation.6 | async-start | bytes 3145728 | tf_op jit(solution)/shard_map/all_to_all | solution.py:36
  565.3 3.7 convolution_convert_fusion.1
  569.0 69.3 %all-to-all-done.5 = bf16[16,2,1,12,2048]{4,1,3,2,0:T(2,128)(2,1)S(1)} async-done(((bf16[16,2,1,12,2048]{4,1,3,2,0:T(2,128)(2,1)}), bf16[16,2,1,12,2048]{4,1,3,2,0:T(2,128)(2,1)S(1)}, u32[]{:S(2)}, u32[]{:S(2)}) %all-to-all-start.5) | async-done | bytes 1572896 | tf_op jit(solution)/shard_map/all_to_all | solution.py:36
  (239 shorter events, 157.9 us)
Async XLA Ops:
  8.0 273.5 %copy-start = (bf16[1,256,2048]{2,1,0:T(8,128)(2,1)S(1)}, bf16[1,256,2048]{2,1,0:T(8,128)(2,1)}, u32[]{:S(2)}) copy-start(bf16[1,256,2048]{2,1,0:T(8,128)(2,1)} %param.34) | copy-start | bytes 3145732
  8.1 331.2 %all-gather.2.cloned.1.call-start = ((), (), s32[]{:S(2)}) async-start(), calls=%async_computation.7 | async-start | bytes 12976128 | tf_op jit(solution)/shard_map/all_gather | solution.py:17
  23.4 32.2 %copy-start.5 = (bf16[128,2048]{1,0:T(8,128)(2,1)S(1)}, bf16[128,2048]{1,0:T(8,128)(2,1)}, u32[]{:S(2)}) copy-start(bf16[128,2048]{1,0:T(8,128)(2,1)} %param.28) | copy-start | bytes 1572868
  23.4 32.2 %copy-start.8 = (f32[2048]{0:T(1024)S(1)}, f32[2048]{0:T(1024)}, u32[]{:S(2)}) copy-start(f32[2048]{0:T(1024)} %param.29) | copy-start | bytes 24580
  31.3 113.2 %all-to-all-start.2 = ((bf16[16,2,1,1,12,2048]{5,1,4,3,2,0:T(2,128)(2,1)}), bf16[16,2,1,1,12,2048]{5,1,4,3,2,0:T(2,128)(2,1)}, u32[]{:S(2)}, u32[]{:S(2)}) async-start(bf16[16,2,1,1,12,2048]{5,1,4,3,2,0:T(2,128)(2,1)} %copy.87), calls=%async_computation.2 | async-start | bytes 3145728 | tf_op jit(solution)/shard_map/all_to_all | solution.py:36
  154.2 6.2 copy-start.6
  154.2 6.4 copy-start.7
  154.2 99.1 %all-to-all-start.3 = ((bf16[4,1,512,2048]{3,2,1,0:T(8,128)(2,1)}), bf16[4,1,512,2048]{3,2,1,0:T(8,128)(2,1)}, u32[]{:S(2)}, u32[]{:S(2)}) async-start(bf16[4,1,512,2048]{3,2,1,0:T(8,128)(2,1)} %stack.2), calls=%async_computation.3 | async-start | bytes 16777216 | tf_op jit(solution)/shard_map/all_to_all | solution.py:175
  160.1 373.7 %reduce-scatter.2.cloned.1.call-start = ((), (), s32[]{:S(2)}) async-start(), calls=%async_computation.8 | async-start | bytes 10485760 | tf_op jit(solution)/shard_map/reduce_scatter | solution.py:203
  259.8 10.4 %copy-start.12 = (bf16[1,2048,256]{2,1,0:T(8,128)(2,1)S(1)}, bf16[1,2048,256]{2,1,0:T(8,128)(2,1)}, u32[]{:S(2)}) copy-start(bf16[1,2048,256]{2,1,0:T(8,128)(2,1)} %param.32) | copy-start | bytes 3145732
  298.3 10.4 %copy-start.13 = (bf16[2048,128]{1,0:T(8,128)(2,1)S(1)}, bf16[2048,128]{1,0:T(8,128)(2,1)}, u32[]{:S(2)}) copy-start(bf16[2048,128]{1,0:T(8,128)(2,1)} %param.35) | copy-start | bytes 1572868
  298.3 12.7 %copy-start.14 = (bf16[128,2048]{1,0:T(8,128)(2,1)S(1)}, bf16[128,2048]{1,0:T(8,128)(2,1)}, u32[]{:S(2)}) copy-start(bf16[128,2048]{1,0:T(8,128)(2,1)} %param.37) | copy-start | bytes 1572868
  298.3 12.7 %copy-start.15 = (bf16[2048,128]{1,0:T(8,128)(2,1)S(1)}, bf16[2048,128]{1,0:T(8,128)(2,1)}, u32[]{:S(2)}) copy-start(bf16[2048,128]{1,0:T(8,128)(2,1)} %param.36) | copy-start | bytes 1572868
  414.6 118.0 %copy-start.10 = (f32[2]{0:T(128)S(1)}, f32[2]{0:T(128)}, u32[]{:S(2)}) copy-start(f32[2]{0:T(128)} %param.25) | copy-start | bytes 28
  414.6 118.2 %copy-start.11 = (f32[128]{0:T(128)S(1)}, f32[128]{0:T(128)}, u32[]{:S(2)}) copy-start(f32[128]{0:T(128)} %param.26) | copy-start | bytes 1540
  416.6 2.9 copy-start.2
  424.7 3.8 copy-start.3
  431.4 2.9 copy-start.2
  439.5 3.8 copy-start.3
  446.1 2.9 copy-start.2
  454.2 3.8 copy-start.3
  460.8 2.9 copy-start.2
  468.9 3.8 copy-start.3
  483.6 3.8 copy-start.3
  490.3 2.9 copy-start.2
  498.3 3.8 copy-start.3
  513.1 3.8 copy-start.3
  527.8 3.8 copy-start.3
  539.8 25.3 %copy-start.9 = (f32[128,2]{0,1:T(2,128)S(1)}, f32[128,2]{0,1:T(2,128)}, u32[]{:S(2)}) copy-start(f32[128,2]{0,1:T(2,128)} %param.31) | copy-start | bytes 3076
  544.8 9.9 %all-to-all-start = ((bf16[4,96,256]{2,1,0:T(8,128)(2,1)}), bf16[4,96,256]{2,1,0:T(8,128)(2,1)S(1)}, u32[]{:S(2)}, u32[]{:S(2)}) async-start(bf16[4,96,256]{2,1,0:T(8,128)(2,1)} %all_to_all.29), calls=%async_computation | async-start | bytes 393216 | tf_op jit(solution)/shard_map/all_to_all | solution.py:142
  554.8 83.5 %all-to-all-start.5 = ((bf16[16,2,1,12,2048]{4,1,3,2,0:T(2,128)(2,1)}), bf16[16,2,1,12,2048]{4,1,3,2,0:T(2,128)(2,1)S(1)}, u32[]{:S(2)}, u32[]{:S(2)}) async-start(bf16[16,2,1,12,2048]{4,1,3,2,0:T(2,128)(2,1)} %copy.96), calls=%async_computation.6 | async-start | bytes 3145728 | tf_op jit(solution)/shard_map/all_to_all | solution.py:36
  642.9 9.9 %copy-start.1 = (bf16[1,256,2048]{2,1,0:T(8,128)(2,1)S(1)}, bf16[1,256,2048]{2,1,0:T(8,128)(2,1)}, u32[]{:S(2)}) copy-start(bf16[1,256,2048]{2,1,0:T(8,128)(2,1)} %param.34) | copy-start | bytes 3145732
  (11 other events, 25.8 us)
Sparse Core Ops, SparseCore 0:
  11.3 165.8 all-gather.1
Sparse Core Ops, SparseCore 1:
  339.4 83.5 reduce-scatter.1
